TPU v7x, 32 devices: a whole 2x2x4 slice. The times are simulated.
32 devices in a mesh: kv: 8 (over z, x), tp: 4 (over y, core).
Axes of the slice: x: 2, y: 2, z: 4, core: 2. Of those that a mesh axis runs over, the one named last changes fastest.
Arguments:
- tokens: bfloat16 [16, 4096], P(None, ('kv', 'tp')), may hold values from -24 to 24
- live_lengths: int32 [16], replicated, may hold values from 64 to 4096, as said below
- kv_cache: bfloat16 [16, 4096, 2048], P(None, 'kv', 'tp'), may hold values from -128 to 128
- gate_sums: float32 [16, 16, 4096], P(None, 'tp', 'kv'), may hold values from -4096 to 0, as said below
- w_query: bfloat16 [4096, 4096], P('kv', 'tp'), may hold values from -0.09375 to 0.09375
- w_key: bfloat16 [4096, 1024], P('kv', 'tp'), may hold values from -0.09375 to 0.09375
- w_value: bfloat16 [4096, 1024], P('kv', 'tp'), may hold values from -0.09375 to 0.09375
- w_forget: bfloat16 [4096, 16], replicated, may hold values from -0.09375 to 0.09375
- forget_bias: float32 [16], replicated, may hold values from -1 to 2
- w_out: bfloat16 [4096, 4096], P('tp', 'kv'), may hold values from -0.5 to 0.5
- first_gain: float32 [4096], P(('kv', 'tp')), may hold values from 0 to 4
- w_gate: bfloat16 [4096, 11264], P('kv', 'tp'), may hold values from -0.09375 to 0.09375
- w_up: bfloat16 [4096, 11264], P('kv', 'tp'), may hold values from -0.09375 to 0.09375
- w_down: bfloat16 [11264, 4096], P('tp', 'kv'), may hold values from -0.078125 to 0.078125
- second_gain: float32 [4096], P(('kv', 'tp')), may hold values from 0 to 4
Outputs:
- layer_out: bfloat16 [16, 4096], P(None, ('kv', 'tp'))
Inputs may be any that keep to these rules, and one draw needn't show every extreme that they name: `live_lengths`: at least one sequence has length exactly 4096. `gate_sums`: entries at positions at or beyond the sequence's length are 0.
All inputs are finite; a program needn't handle non-finite values.
Results may differ from a plain program's by a relative error of at most 0.019.
Values may be sent and summed in bfloat16 or wider, within the bound.
A program may use at most 64 MiB of HBM per device.

v0:
```python
import jax
import jax.numpy as jnp
from jax import lax
from jax.sharding import PartitionSpec as P

D = 4096
DH = 64
GROUP = 4


EPSILON = 1e-05
EMPTY_SCORE = -1e30


def combined_all(shard, axis, combine):
    everything = jax.tree.map(lambda part: lax.all_gather(part, axis), shard)
    initial = jax.tree.map(lambda part: part[0], everything)

    def lap(k, so_far):
        return combine(so_far, jax.tree.map(lambda part: part[k], everything))

    return lax.fori_loop(1, lax.axis_size(axis), lap, initial)


def combine_parts(earlier, later):
    earlier_top, earlier_total, earlier_sum = earlier
    later_top, later_total, later_sum = later
    joint_top = jnp.maximum(earlier_top, later_top)
    earlier_scale = jnp.exp(earlier_top - joint_top)
    later_scale = jnp.exp(later_top - joint_top)
    joint_total = earlier_total * earlier_scale + later_total * later_scale
    joint_sum = earlier_sum * earlier_scale[..., None] + later_sum * later_scale[..., None]
    return (joint_top, joint_total, joint_sum)


def normalize_block(mixture, norm_gain):
    row_sum, row_square = lax.psum(
        (jnp.sum(mixture, axis=1), jnp.sum(mixture * mixture, axis=1)), "kv"
    )
    centre = row_sum / D
    spread = row_square / D - centre * centre
    scaled = (mixture - centre[:, None]) * lax.rsqrt(spread[:, None] + EPSILON) * norm_gain
    return scaled.astype(jnp.bfloat16)


def on_device(
    tokens,
    live_lengths,
    kv_cache,
    gate_sums,
    w_query,
    w_key,
    w_value,
    w_forget,
    forget_bias,
    w_out,
    first_gain,
    w_gate,
    w_up,
    w_down,
    second_gain,
):
    sequences = tokens.shape[0]
    own_cols = tokens.shape[1]
    gains_pair = jnp.stack([first_gain, second_gain], axis=0)
    wide_rows, wide_gains = (
        lax.all_gather(tokens.astype(jnp.float32), "tp", axis=1, tiled=True),
        lax.all_gather(gains_pair, "tp", axis=1, tiled=True),
    )
    block_rows = wide_rows.astype(jnp.bfloat16)
    row_count = block_rows.shape[1]
    row_start = lax.axis_index("kv") * row_count
    local_heads = kv_cache.shape[2] // (2 * DH)
    head_start = lax.axis_index("tp") * local_heads
    forget_rows = lax.dynamic_slice(w_forget, (row_start, head_start), (row_count, local_heads))
    query_part = jnp.dot(block_rows, w_query, preferred_element_type=jnp.float32)
    key_part = jnp.dot(block_rows, w_key, preferred_element_type=jnp.float32)
    value_part = jnp.dot(block_rows, w_value, preferred_element_type=jnp.float32)
    forget_part = jnp.dot(block_rows, forget_rows, preferred_element_type=jnp.float32)
    query_sum, key_sum, value_sum, forget_sum = lax.psum(
        (query_part, key_part, value_part, forget_part), "kv"
    )
    queries = query_sum.astype(jnp.bfloat16).reshape(sequences, local_heads, GROUP, DH)
    new_keys = key_sum.astype(jnp.bfloat16).reshape(sequences, local_heads, DH)
    new_values = value_sum.astype(jnp.bfloat16).reshape(sequences, local_heads, DH)
    bias_rows = lax.dynamic_slice_in_dim(forget_bias, head_start, local_heads)
    new_gate = jax.nn.log_sigmoid(forget_sum + bias_rows)
    positions = kv_cache.shape[1]
    cached = kv_cache.reshape(sequences, positions, local_heads, 2, DH)
    score_scale = DH ** (-0.5)
    scores = (
        jnp.einsum(
            "bgjd,bpgd->bgjp", queries, cached[:, :, :, 0], preferred_element_type=jnp.float32
        )
        * score_scale
    )
    scores = scores + gate_sums[:, :, None, :] + new_gate[:, :, None, None]
    position_selector = lax.axis_index("kv") * positions + jnp.arange(positions, dtype=jnp.int32)
    live_mask = (position_selector[None, :] < live_lengths[:, None])[:, None, None, :]
    local_top = jnp.max(jnp.where(live_mask, scores, EMPTY_SCORE), axis=-1)
    weights = jnp.where(live_mask, jnp.exp(scores - local_top[..., None]), 0.0)
    local_total = jnp.sum(weights, axis=-1)
    local_sum = jnp.einsum(
        "bgjp,bpgd->bgjd",
        weights.astype(jnp.bfloat16),
        cached[:, :, :, 1],
        preferred_element_type=jnp.float32,
    )
    row_top, weight_total, summed = combined_all(
        (local_top, local_total, local_sum), "kv", combine_parts
    )
    own_score = (
        jnp.einsum("bgjd,bgd->bgj", queries, new_keys, preferred_element_type=jnp.float32)
        * score_scale
    )
    final_top = jnp.maximum(row_top, own_score)
    carry_scale = jnp.exp(row_top - final_top)
    own_weight = jnp.exp(own_score - final_top)
    own_rounded = lax.optimization_barrier(own_weight.astype(jnp.bfloat16)).astype(jnp.float32)
    numerator = summed * carry_scale[..., None] + own_rounded[..., None] * new_values[
        :, :, None, :
    ].astype(jnp.float32)
    attended = (numerator / (weight_total * carry_scale + own_weight)[..., None]).astype(
        jnp.bfloat16
    )
    attended = attended.reshape(sequences, local_heads * GROUP * DH)
    attn_part = jnp.dot(attended, w_out, preferred_element_type=jnp.float32)
    attn_block = lax.psum(attn_part, "tp")
    mid_rows = normalize_block(wide_rows + attn_block, wide_gains[0])
    gate_part = jnp.dot(mid_rows, w_gate, preferred_element_type=jnp.float32)
    up_part = jnp.dot(mid_rows, w_up, preferred_element_type=jnp.float32)
    gate_full, up_full = (
        lax.psum(gate_part.astype(jnp.bfloat16), "kv").astype(jnp.float32),
        lax.psum(up_part.astype(jnp.bfloat16), "kv").astype(jnp.float32),
    )
    hidden = (jax.nn.silu(gate_full) * up_full).astype(jnp.bfloat16)
    ffn_part = jnp.dot(hidden, w_down, preferred_element_type=jnp.float32)
    ffn_block = lax.psum(ffn_part, "tp")
    out_block = normalize_block(mid_rows.astype(jnp.float32) + ffn_block, wide_gains[1])
    return lax.dynamic_slice_in_dim(out_block, lax.axis_index("tp") * own_cols, own_cols, 1)


def solution(mesh):
    in_specs = (
        P(None, ("kv", "tp")),
        P(),
        P(None, "kv", "tp"),
        P(None, "tp", "kv"),
        P("kv", "tp"),
        P("kv", "tp"),
        P("kv", "tp"),
        P(),
        P(),
        P("tp", "kv"),
        P(("kv", "tp")),
        P("kv", "tp"),
        P("kv", "tp"),
        P("tp", "kv"),
        P(("kv", "tp")),
    )
    out_specs = P(None, ("kv", "tp"))
    return jax.shard_map(
        on_device, mesh=mesh, in_specs=in_specs, out_specs=out_specs, check_vma=False
    )
```

profile of v0, /device:TPU:0, one launch (start us, length us, event | category | flops | bytes accessed | tf_op | source)
XLA Modules:
  0.0 333.8 jit_solution(3418415912000311669)
XLA Ops:
  6.5 0.8 convert_element_type.62
  7.4 6.4 %all_gather.24 = f32[16,512]{1,0:T(8,128)S(1)} all-gather(f32[16,128]{1,0:T(8,128)S(1)} %convert_element_type.62), channel_id=1, replica_groups=mesh['kv'=8,'tp'=4] {'tp'}, dimensions={1}, use_global_device_ids=true | all-gather | bytes 40960 | tf_op jit(solution)/shard_map/all_gather | solution.py:67
  13.8 1.1 fusion.40
  14.9 1.1 fusion.38
  16.0 1.5 fusion.37
  18.2 0.9 convolution_bitcast_fusion
  19.1 39.2 %all-reduce.2 = (bf16[16,1024]{1,0:T(8,128)(2,1)S(1)}, f32[16,4]{0,1:T(4,128)S(1)}, bf16[16,256]{1,0:T(8,128)(2,1)S(1)}, bf16[16,256]{1,0:T(8,128)(2,1)S(1)}) all-reduce(f32[16,1024]{1,0:T(8,128)S(1)} %fusion.37, f32[16,4]{0,1:T(4,128)S(1)} %convolution_bitcast_fusion, ...), channel_id=1, replica_groups=mesh['kv'=8,'tp'=4] {'kv'}, use_global_device_ids=true, to_apply=%region_0.0 | all-reduce | flops 24640 | bytes 147968 | tf_op jit(solution)/shard_map/psum | solution.py:80
  58.5 12.3 %copy.37 = bf16[16,512,512]{1,2,0:T(8,128)(2,1)} copy(bf16[16,512,512]{2,1,0:T(8,128)(2,1)} %param.19) | data formatting | bytes 16777216 | tf_op args[2]
  71.0 3.0 select_reduce_fusion
  74.0 3.5 %fusion.3 = f32[16,4,4,64]{3,2,1,0:T(4,128)S(1)} fusion(bf16[16,512,4,2,64]{1,4,3,2,0:T(8,128)(2,1)} %bitcast.77, f32[16,4,4,512]{3,2,1,0:T(4,128)S(1)} %get-tuple-element.244, f32[16,4,4]{2,1,0:T(4,128)S(1)} %get-tuple-element.243, pred[16,512]{1,0:T(8,128)(4,1)S(1)} %broadcast_compare_fusion), kind=kOutput, calls=%fused_computation.9 | convolution fusion | flops 17170432 | bytes 4793344 | tf_op jit(solution)/shard_map/bgjp,bpgd->bgjd/dot_general | solution.py:103
  77.9 30.8 %all-gather = f32[128,4,4]{2,1,0:T(4,128)S(1)} all-gather(f32[16,4,4]{2,1,0:T(4,128)S(1)} %get-tuple-element.243), channel_id=2, replica_groups=mesh['kv'=8,'tp'=4] {'kv'}, dimensions={0}, use_global_device_ids=true | all-gather | bytes 9216 | tf_op jit(solution)/shard_map/all_gather | solution.py:16
  108.7 5.1 %all_gather.31 = f32[2,512]{1,0:T(2,128)S(1)} all-gather(f32[2,128]{1,0:T(2,128)S(1)} %pad_maximum_fusion), channel_id=1, replica_groups=mesh['kv'=8,'tp'=4] {'tp'}, dimensions={1}, use_global_device_ids=true | all-gather | bytes 5120 | tf_op jit(solution)/shard_map/all_gather | solution.py:68
  114.6 30.9 %all-gather.1 = f32[128,4,4]{2,1,0:T(4,128)S(1)} all-gather(f32[16,4,4]{2,1,0:T(4,128)S(1)} %fusion.9), channel_id=3, replica_groups=mesh['kv'=8,'tp'=4] {'kv'}, dimensions={0}, use_global_device_ids=true | all-gather | bytes 9216 | tf_op jit(solution)/shard_map/all_gather | solution.py:16
  145.8 33.3 %all-gather.2 = f32[128,4,4,64]{3,2,1,0:T(4,128)S(1)} all-gather(f32[16,4,4,64]{3,2,1,0:T(4,128)S(1)} %fusion.3), channel_id=4, replica_groups=mesh['kv'=8,'tp'=4] {'kv'}, dimensions={0}, use_global_device_ids=true | all-gather | bytes 589824 | tf_op jit(solution)/shard_map/all_gather | solution.py:16
  179.2 1.0 copy-done.1
  180.1 11.1 %while.19 = (s32[]{:T(128)}, f32[16,4,4]{0,2,1:T(4,128)S(1)}, f32[16,4,4]{0,2,1:T(4,128)S(1)}, f32[16,4,4,64]{3,2,1,0:T(4,128)S(1)}, f32[8,16,4,4]{1,3,2,0:T(4,1...) while((s32[]{:T(128)}, f32[16,4,4]{0,2,1:T(4,128)S(1)}, ...), condition=%wide.region_5.6_spmd, body=%wide.region_4.5_spmd.sunk | while | flops 50693 | bytes 211087 | solution.py:22
  180.4 1.3 fusion.62
  182.0 1.3 fusion.62
  183.6 1.3 fusion.62
  185.1 1.3 fusion.62
  186.7 1.3 fusion.62
  188.3 1.3 fusion.62
  189.9 1.3 fusion.62
  192.0 1.5 fusion.41
  193.5 10.3 %psum.88 = f32[16,512]{1,0:T(8,128)S(1)} all-reduce(f32[16,512]{1,0:T(8,128)S(1)} %fusion.41), channel_id=1, replica_groups=mesh['kv'=8,'tp'=4] {'tp'}, use_global_device_ids=true, to_apply=%region_8.9 | all-reduce | flops 8192 | bytes 65536 | tf_op jit(solution)/shard_map/psum | solution.py:128
  203.9 17.5 %all-reduce.1 = (f32[16]{0:T(128)S(1)}, f32[16]{0:T(128)S(1)}) all-reduce(f32[16]{0:T(128)S(1)} %get-tuple-element.203, f32[16]{0:T(128)S(1)} %get-tuple-element.202), channel_id=1, replica_groups=mesh['kv'=8,'tp'=4] {'kv'}, use_global_device_ids=true, to_apply=%region_12.13 | all-reduce | flops 32 | bytes 256 | tf_op jit(solution)/shard_map/psum | solution.py:37
  221.3 1.2 convolution_convert_fusion.1
  223.2 1.2 convolution_convert_fusion
  224.4 69.4 %all-reduce.6.cloned.1.call-done = (bf16[16,2816]{1,0:T(8,128)(2,1)}, bf16[16,2816]{1,0:T(8,128)(2,1)}) async-done(((bf16[16,2816]{1,0:T(8,128)(2,1)}, bf16[16,2816]{1,0:T(8,128)(2,1)}), (bf16[16,2816]{1,0:T(8,128)(2,1)}, bf16[16,2816]{1,0:T(8,128)(2,1)})) %all-reduce.6.cloned.1.call-update) | async-done | bytes 180240 | tf_op jit(solution)/shard_map/psum | solution.py:134
  293.8 2.4 fusion.20
  296.2 10.3 %psum.93 = f32[16,512]{1,0:T(8,128)S(1)} all-reduce(f32[16,512]{1,0:T(8,128)S(1)} %fusion.20), channel_id=1, replica_groups=mesh['kv'=8,'tp'=4] {'tp'}, use_global_device_ids=true, to_apply=%region_15.16 | all-reduce | flops 8192 | bytes 65536 | tf_op jit(solution)/shard_map/psum | solution.py:138
  306.7 19.6 %all-reduce = (f32[16]{0:T(128)S(1)}, f32[16]{0:T(128)S(1)}) all-reduce(f32[16]{0:T(128)S(1)} %get-tuple-element.201, f32[16]{0:T(128)S(1)} %get-tuple-element.200), channel_id=1, replica_groups=mesh['kv'=8,'tp'=4] {'kv'}, use_global_device_ids=true, to_apply=%region_19.20 | all-reduce | flops 32 | bytes 256 | tf_op jit(solution)/shard_map/psum | solution.py:37
  (69 shorter events, 7.0 us)
Async XLA Ops:
  6.5 214.8 %copy-start = (bf16[512,2816]{1,0:T(8,128)(2,1)S(1)}, bf16[512,2816]{1,0:T(8,128)(2,1)}, u32[]{:S(2)}) copy-start(bf16[512,2816]{1,0:T(8,128)(2,1)} %param.28) | copy-start | bytes 8650756
  6.5 287.3 %all-reduce.6.cloned.1.call-start = ((), (), s32[]{:S(2)}) async-start(), calls=%async_computation | async-start | bytes 360448 | tf_op jit(solution)/shard_map/psum | solution.py:134
  58.5 12.4 %copy-start.5 = (s32[16]{0:T(128)S(1)}, s32[16]{0:T(128)}, u32[]{:S(2)}) copy-start(s32[16]{0:T(128)} %param.18) | copy-start | bytes 196
  58.5 12.4 %copy-start.6 = (f32[16,4,512]{2,1,0:T(4,128)S(1)}, f32[16,4,512]{2,1,0:T(4,128)}, u32[]{:S(2)}) copy-start(f32[16,4,512]{2,1,0:T(4,128)} %param.20) | copy-start | bytes 393220
  74.0 34.7 %copy-start.3 = (f32[128]{0:T(128)S(1)}, f32[128]{0:T(128)}, u32[]{:S(2)}) copy-start(f32[128]{0:T(128)} %param.31) | copy-start | bytes 1540
  74.0 34.7 %copy-start.4 = (f32[128]{0:T(128)S(1)}, f32[128]{0:T(128)}, u32[]{:S(2)}) copy-start(f32[128]{0:T(128)} %param.27) | copy-start | bytes 1540
  179.1 1.0 copy-start.1
  221.3 1.8 copy-start.2
Sparse Core Ops, SparseCore 0:
  224.5 69.3 all-reduce.5
where the time goes:
time: 335 us; the launch traced here: 334 us
  blocking collectives  203 us (61%)
  waiting for transfers between devices  69.4 us (21%)
  local copies, waits for them, and re-layouts  18 us (5%)
  matrix products  17.4 us (5%)
  between operations  13.5 us (4%)
  other arithmetic  12.2 us (4%)
    all_gather x3, blocking collectives, combined_all(): everything = jax.tree.map(lambda part: lax.all_gather(part, axis), shard)  94.9 us
    psum x1, waiting for transfers between devices, on_device(): lax.psum(up_part.astype(jnp.bfloat16), 'kv').astype(jnp.float32)  69.4 us
    psum x1, blocking collectives, on_device(): lax.psum((query_part, key_part, value_part, forget_part), 'kv')  39.2 us
    psum x2, blocking collectives, normalize_block(): lax.psum((jnp.sum(mixture, axis=1), jnp.sum(mixture * mixture, axis=1)),...  37 us
    unnamed x15, local copies, waits for them, and re-layouts  14 us
    psum x1, blocking collectives, on_device(): attn_block = lax.psum(attn_part, 'tp')  10.3 us
    psum x1, blocking collectives, on_device(): ffn_block = lax.psum(ffn_part, 'tp')  10.3 us
    add x7, other arithmetic, combine_parts(): earlier_sum * earlier_scale[..., None] + later_sum * later_scale[..., None]  9.26 us
  transfers between devices with their start and end apart: 1, of which 1 were waited for; matrix products, arithmetic and copies ran while one was open for 0% of the time, Pallas kernels for 0%

commit v1 on v0

--- a/solution.py
+++ b/solution.py
@@ -1,6 +1,10 @@
+import functools
+
 import jax
 import jax.numpy as jnp
 from jax import lax
+from jax.experimental import pallas as pl
+from jax.experimental.pallas import tpu as pltpu
 from jax.sharding import PartitionSpec as P
 
 D = 4096
@@ -140,6 +144,571 @@
     return lax.dynamic_slice_in_dim(out_block, lax.axis_index("tp") * own_cols, own_cols, 1)
 
 
+MESH = pl.DeviceIdType.MESH
+F32 = jnp.float32
+BF16 = jnp.bfloat16
+LANES = 128
+
+
+def push(axis, peer, me, source, landing, sends, recvs):
+    return pltpu.make_async_remote_copy(
+        src_ref=source,
+        dst_ref=landing.at[me],
+        send_sem=sends.at[peer],
+        recv_sem=recvs.at[me],
+        device_id={axis: peer},
+        device_id_type=MESH,
+    )
+
+
+def arrival(axis, peer, source, landing, sends, recvs):
+    return pltpu.make_async_remote_copy(
+        src_ref=source,
+        dst_ref=landing.at[peer],
+        send_sem=sends.at[peer],
+        recv_sem=recvs.at[peer],
+        device_id={axis: peer},
+        device_id_type=MESH,
+    )
+
+
+def head_rows(block, odd, lane):
+    moved = pltpu.roll(block, DH, 1) if odd else block
+    return jnp.where(lane < DH, moved, 0.0)
+
+
+def fused_kernel(
+    dims,
+    tokens,
+    lengths,
+    cache_hbm,
+    gates_hbm,
+    wq_hbm,
+    wk_hbm,
+    wv_hbm,
+    wf_hbm,
+    bias,
+    wo_hbm,
+    gain_one,
+    wg_hbm,
+    wu_hbm,
+    wd_hbm,
+    gain_two,
+    out,
+    wqkv,
+    wf,
+    cache,
+    gates,
+    wo,
+    wg,
+    wu,
+    wd,
+    tok_own,
+    tok_all,
+    qkv_part,
+    qkv_in,
+    qkv_own,
+    qkv_all,
+    q_rows,
+    kv_rows,
+    gate_now,
+    att_part,
+    att_in,
+    att_own,
+    att_all,
+    x_own,
+    x_in,
+    y_own,
+    y_in,
+    s1_own,
+    s1_in,
+    s2_own,
+    s2_in,
+    gu_part,
+    gu_in,
+    hid_own,
+    hid_all,
+    wide,
+    sems,
+    tp_send,
+    tp_recv,
+    kv_send,
+    kv_recv,
+):
+    seqs, k_size, t_size, heads, chunk, n_chunks, f_chunk, positions = dims
+    kv = lax.axis_index("kv")
+    tp = lax.axis_index("tp")
+    rows_n = wq_hbm.shape[0]
+    q_cols = wq_hbm.shape[1]
+    kk = wk_hbm.shape[1]
+    ff = wg_hbm.shape[1]
+    width = wo_hbm.shape[1]
+    per = seqs // k_size
+    rows = heads * GROUP
+    local = [
+        pltpu.make_async_copy(wq_hbm, wqkv.at[:, :q_cols], sems.at[0]),
+        pltpu.make_async_copy(wk_hbm, wqkv.at[:, q_cols : q_cols + kk], sems.at[1]),
+        pltpu.make_async_copy(wv_hbm, wqkv.at[:, q_cols + kk :], sems.at[2]),
+        pltpu.make_async_copy(
+            wf_hbm.at[pl.ds(pl.multiple_of(kv * rows_n, rows_n), rows_n), :], wf, sems.at[3]
+        ),
+        pltpu.make_async_copy(cache_hbm, cache, sems.at[4]),
+        pltpu.make_async_copy(gates_hbm, gates, sems.at[5]),
+        pltpu.make_async_copy(wo_hbm, wo, sems.at[6]),
+        pltpu.make_async_copy(wg_hbm, wg.at[:, :ff], sems.at[7]),
+        pltpu.make_async_copy(wu_hbm, wu.at[:, :ff], sems.at[8]),
+        pltpu.make_async_copy(wd_hbm, wd.at[:ff, :], sems.at[9]),
+    ]
+    for copy in local:
+        copy.start()
+    barrier = pltpu.get_barrier_semaphore()
+    for i in range(1, k_size):
+        pl.semaphore_signal(
+            barrier, inc=1, device_id={"kv": lax.rem(kv + i, k_size)}, device_id_type=MESH
+        )
+    for i in range(1, t_size):
+        pl.semaphore_signal(
+            barrier, inc=1, device_id={"tp": lax.rem(tp + i, t_size)}, device_id_type=MESH
+        )
+    padded = wg.shape[1]
+    if padded > ff:
+        wg[:, ff:] = jnp.zeros((rows_n, padded - ff), BF16)
+        wu[:, ff:] = jnp.zeros((rows_n, padded - ff), BF16)
+        wd[ff:, :] = jnp.zeros((padded - ff, width), BF16)
+    tok_own[:seqs, :] = tokens[...].astype(F32)
+    tok_own[seqs:, :] = jnp.broadcast_to(gain_one[...], (8, LANES))
+    pl.semaphore_wait(barrier, k_size - 1 + t_size - 1)
+
+    def tp_all(phase, own, landing):
+        s, r = tp_send.at[phase], tp_recv.at[phase]
+        for i in range(1, t_size):
+            push("tp", lax.rem(tp + i, t_size), tp, own, landing, s, r).start()
+        landing[tp] = own[...]
+        for i in range(1, t_size):
+            arrival("tp", lax.rem(tp + i, t_size), own, landing, s, r).wait_recv()
+
+    def kv_all(phase, own, landing):
+        s, r = kv_send.at[phase], kv_recv.at[phase]
+
+        def go(i, c):
+            push("kv", lax.rem(kv + i, k_size), kv, own, landing, s, r).start()
+            return c
+
+        def come(i, c):
+            arrival("kv", lax.rem(kv + i, k_size), own, landing, s, r).wait_recv()
+            return c
+
+        lax.fori_loop(1, k_size, go, 0)
+        landing[kv] = own[...]
+        lax.fori_loop(1, k_size, come, 0)
+
+    tp_all(0, tok_own, tok_all)
+    wide_rows = jnp.concatenate([tok_all[t, :seqs, :] for t in range(t_size)], axis=1)
+    wide_gain = jnp.concatenate([tok_all[t, seqs : seqs + 1, :] for t in range(t_size)], axis=1)
+    wide[...] = wide_rows
+    block = wide_rows.astype(BF16)
+    for n in range(4):
+        local[n].wait()
+    for c in range(n_chunks - 1):
+        qkv_part[c] = jnp.dot(
+            block, wqkv[:, c * chunk : (c + 1) * chunk], preferred_element_type=F32
+        )
+    kv_heads = wf.shape[1]
+    qkv_part[n_chunks - 1] = jnp.zeros((seqs, chunk), F32)
+    qkv_part[n_chunks - 1, :, :kv_heads] = jnp.dot(block, wf[...], preferred_element_type=F32)
+    s, r = kv_send.at[0], kv_recv.at[0]
+    s2, r2 = kv_send.at[1], kv_recv.at[1]
+
+    def qkv_go(i, c):
+        peer = lax.rem(kv + i, k_size)
+
+        @pl.when(peer < n_chunks)
+        def _():
+            push("kv", peer, kv, qkv_part.at[peer], qkv_in, s, r).start()
+
+        return c
+
+    lax.fori_loop(1, k_size, qkv_go, 0)
+
+    @pl.when(kv < n_chunks)
+    def _():
+        qkv_in[kv] = qkv_part[kv]
+
+        def come(i, c):
+            peer = lax.rem(kv + i, k_size)
+            arrival("kv", peer, qkv_part.at[0], qkv_in, s, r).wait_recv()
+            return c
+
+        lax.fori_loop(1, k_size, come, 0)
+        total = qkv_in[0]
+        for k in range(1, k_size):
+            total = total + qkv_in[k]
+        scale = jnp.where(kv < q_cols // chunk, DH**-0.5, 1.0).astype(F32)
+        rounded = total.astype(BF16).astype(F32) * scale
+        exact = jnp.full((seqs, chunk), kv, jnp.int32) == n_chunks - 1
+        qkv_own[...] = jnp.where(exact, total, rounded)
+
+        def go(i, c):
+            push("kv", lax.rem(kv + i, k_size), kv, qkv_own, qkv_all, s2, r2).start()
+            return c
+
+        lax.fori_loop(1, k_size, go, 0)
+        qkv_all[kv] = qkv_own[...]
+
+    def qkv_come(i, c):
+        peer = lax.rem(kv + i, k_size)
+
+        @pl.when(peer < n_chunks)
+        def _():
+            arrival("kv", peer, qkv_own, qkv_all, s2, r2).wait_recv()
+
+        return c
+
+    lax.fori_loop(1, k_size, qkv_come, 0)
+    lane = lax.broadcasted_iota(jnp.int32, (seqs, LANES), 1)
+
+    def unit(start):
+        return qkv_all[start // chunk, :, start % chunk : start % chunk + LANES]
+
+    for h in range(rows):
+        start = h * DH
+        base = start // LANES * LANES
+        q_rows[pl.ds(h, seqs, stride=rows), :] = head_rows(unit(base), start % LANES != 0, lane)
+    for g in range(heads):
+        base = g * DH // LANES * LANES
+        odd = g % 2 == 1
+        keys = unit(q_cols + base)
+        values = unit(q_cols + kk + base)
+        keys = pltpu.roll(keys, DH, 1) if odd else keys
+        values = values if odd else pltpu.roll(values, DH, 1)
+        pair = jnp.where(lane < DH, keys, values)
+        for j in range(GROUP):
+            kv_rows[pl.ds(g * GROUP + j, seqs, stride=rows), :] = pair
+    logits = qkv_all[n_chunks - 1, :, :kv_heads] + bias[...]
+    gate_now[:, :kv_heads] = jnp.minimum(logits, 0.0) - jnp.log(1.0 + jnp.exp(-jnp.abs(logits)))
+    local[4].wait()
+    local[5].wait()
+    row_p = lax.broadcasted_iota(jnp.int32, (rows, positions), 0) // GROUP
+    pos = lax.broadcasted_iota(jnp.int32, (rows, positions), 1) + kv * positions
+    row_l = lax.broadcasted_iota(jnp.int32, (rows, LANES), 0) // GROUP
+    lane_l = lax.broadcasted_iota(jnp.int32, (rows, LANES), 1)
+    row_g = lax.broadcasted_iota(jnp.int32, (rows, kv_heads), 0) // GROUP
+    lane_g = lax.broadcasted_iota(jnp.int32, (rows, kv_heads), 1)
+
+    def attend(b):
+        q = q_rows[pl.ds(pl.multiple_of(b * rows, rows), rows), :]
+        spread = jnp.concatenate(
+            [jnp.where(row_l == g, q, 0.0).astype(BF16) for g in range(heads)], axis=1
+        )
+        slab = cache[b]
+        scores = lax.dot_general(
+            spread, slab, (((1,), (1,)), ((), ())), preferred_element_type=F32
+        )
+        gate_rows = gates[b]
+        gate = jnp.broadcast_to(gate_rows[0:1], (rows, positions))
+        for g in range(1, heads):
+            gate = jnp.where(row_p == g, gate_rows[g : g + 1], gate)
+        fresh = jnp.sum(
+            jnp.where(lane_g == row_g + tp * heads, gate_now[pl.ds(b, 1), :kv_heads], 0.0),
+            axis=1,
+            keepdims=True,
+        )
+        scores = scores + gate + fresh
+        live = pos < lengths[b]
+        scores = jnp.where(live, scores, EMPTY_SCORE)
+        top = jnp.max(scores, axis=1, keepdims=True)
+        weights = jnp.where(live, jnp.exp(scores - top), 0.0)
+        total = jnp.sum(weights, axis=1, keepdims=True)
+        mixed = jnp.dot(weights.astype(BF16), slab, preferred_element_type=F32)
+        own = mixed[:, :LANES]
+        for g in range(1, heads):
+            own = jnp.where(row_l == g, mixed[:, g * LANES : (g + 1) * LANES], own)
+        own = jnp.where(lane_l < DH // 2, top, jnp.where(lane_l < DH, total, own))
+        return own
+
+    sa, ra = kv_send.at[2], kv_recv.at[2]
+
+    def att_go(i, c):
+        peer = lax.rem(kv + i, k_size)
+        for e in range(per):
+            att_part[peer, e] = attend(peer * per + e)
+
+        @pl.when(i < k_size)
+        def _():
+            push("kv", peer, kv, att_part.at[peer], att_in, sa, ra).start()
+
+        return c
+
+    lax.fori_loop(1, k_size + 1, att_go, 0)
+    att_in[kv] = att_part[kv]
+
+    def att_come(i, c):
+        arrival("kv", lax.rem(kv + i, k_size), att_part.at[0], att_in, sa, ra).wait_recv()
+        return c
+
+    lax.fori_loop(1, k_size, att_come, 0)
+    for e in range(per):
+        at = pl.ds(pl.multiple_of((kv * per + e) * rows, rows), rows)
+        q, pair = q_rows[at, :], kv_rows[at, :]
+        own_score = jnp.sum(jnp.where(lane_l < DH, q * pair, 0.0), axis=1, keepdims=True)
+        parts = [att_in[k, e] for k in range(k_size)]
+        tops = [part[:, 0:1] for part in parts]
+        high = own_score
+        for top in tops:
+            high = jnp.maximum(high, top)
+        own_weight = jnp.exp(own_score - high)
+        numer = own_weight.astype(BF16).astype(F32) * pair
+        denom = own_weight
+        for top, part in zip(tops, parts):
+            scale = jnp.exp(top - high)
+            numer = numer + part * scale
+            denom = denom + part[:, DH // 2 : DH // 2 + 1] * scale
+        att_own[pl.ds(e * rows, rows), :] = jnp.where(lane_l < DH, 0.0, numer / denom)
+    kv_all(3, att_own, att_all)
+    for k in range(k_size):
+        q_rows[k * per * rows : (k + 1) * per * rows, :] = att_all[k]
+    pieces = []
+    for h in range(0, rows, 2):
+        even = pltpu.roll(q_rows[pl.ds(h, seqs, stride=rows), :], DH, 1)
+        odd = q_rows[pl.ds(h + 1, seqs, stride=rows), :]
+        pieces.append(jnp.where(lane < DH, even, odd).astype(BF16))
+    attended = jnp.concatenate(pieces, axis=1)
+    local[6].wait()
+    x_own[...] = jnp.dot(attended, wo[...], preferred_element_type=F32)
+
+    def normed(z, phase, stat_own, stat_in):
+        row_sum = jnp.sum(z, axis=1, keepdims=True)
+        row_square = jnp.sum(z * z, axis=1, keepdims=True)
+        stat_own[...] = jnp.where(lane == 0, row_sum, row_square)
+        kv_all(phase, stat_own, stat_in)
+        stats = stat_in[0]
+        for k in range(1, k_size):
+            stats = stats + stat_in[k]
+        count = k_size * width
+        centre = stats[:, 0:1] / count
+        spread = stats[:, 1:2] / count - centre * centre
+        return (z - centre) * lax.rsqrt(spread + EPSILON)
+
+    tp_all(1, x_own, x_in)
+    z = wide[...]
+    for t in range(t_size):
+        z = z + x_in[t]
+    mid = (normed(z, 4, s1_own, s1_in) * wide_gain).astype(BF16)
+    local[7].wait()
+    local[8].wait()
+    sg, rg = kv_send.at[5], kv_recv.at[5]
+
+    def gu_go(i, c):
+        peer = lax.rem(kv + i, k_size)
+        at = pl.ds(pl.multiple_of(peer * f_chunk, LANES), f_chunk)
+        gu_part[peer, 0] = jnp.dot(mid, wg[:, at], preferred_element_type=F32).astype(BF16)
+        gu_part[peer, 1] = jnp.dot(mid, wu[:, at], preferred_element_type=F32).astype(BF16)
+
+        @pl.when(i < k_size)
+        def _():
+            push("kv", peer, kv, gu_part.at[peer], gu_in, sg, rg).start()
+
+        return c
+
+    lax.fori_loop(1, k_size + 1, gu_go, 0)
+    gu_in[kv] = gu_part[kv]
+
+    def gu_come(i, c):
+        arrival("kv", lax.rem(kv + i, k_size), gu_part.at[0], gu_in, sg, rg).wait_recv()
+        return c
+
+    lax.fori_loop(1, k_size, gu_come, 0)
+    gate = gu_in[0, 0].astype(F32)
+    up = gu_in[0, 1].astype(F32)
+    for k in range(1, k_size):
+        gate = gate + gu_in[k, 0].astype(F32)
+        up = up + gu_in[k, 1].astype(F32)
+    hid_own[...] = (gate / (1.0 + jnp.exp(-gate)) * up).astype(BF16)
+    local[9].wait()
+    sh, rh = kv_send.at[6], kv_recv.at[6]
+
+    def hid_go(i, c):
+        push("kv", lax.rem(kv + i, k_size), kv, hid_own, hid_all, sh, rh).start()
+        return c
+
+    lax.fori_loop(1, k_size, hid_go, 0)
+    hid_all[kv] = hid_own[...]
+
+    def down(i, acc):
+        peer = lax.rem(kv + i, k_size)
+
+        @pl.when(i > 0)
+        def _():
+            arrival("kv", peer, hid_own, hid_all, sh, rh).wait_recv()
+
+        at = pl.ds(pl.multiple_of(peer * f_chunk, LANES), f_chunk)
+        return acc + jnp.dot(hid_all[peer], wd[at, :], preferred_element_type=F32)
+
+    y_own[...] = lax.fori_loop(0, k_size, down, jnp.zeros((seqs, width), F32))
+    tp_all(2, y_own, y_in)
+    z = mid.astype(F32)
+    for t in range(t_size):
+        z = z + y_in[t]
+    wide[...] = normed(z, 7, s2_own, s2_in)
+    mine = wide[:, pl.ds(pl.multiple_of(tp * LANES, LANES), LANES)]
+    out[...] = (mine * gain_two[...]).astype(BF16)
+
+    for phase, own, landing in ((0, tok_own, tok_all), (1, x_own, x_in), (2, y_own, y_in)):
+        for i in range(1, t_size):
+            peer = lax.rem(tp + i, t_size)
+            arrival("tp", peer, own, landing, tp_send.at[phase], tp_recv.at[phase]).wait_send()
+
+    def finish(i, c):
+        peer = lax.rem(kv + i, k_size)
+
+        @pl.when(peer < n_chunks)
+        def _():
+            arrival("kv", peer, qkv_part.at[peer], qkv_in, s, r).wait_send()
+
+        @pl.when(kv < n_chunks)
+        def _():
+            arrival("kv", peer, qkv_own, qkv_all, s2, r2).wait_send()
+
+        for phase, own, landing in (
+            (2, att_part.at[peer], att_in),
+            (3, att_own, att_all),
+            (4, s1_own, s1_in),
+            (5, gu_part.at[peer], gu_in),
+            (6, hid_own, hid_all),
+            (7, s2_own, s2_in),
+        ):
+            arrival("kv", peer, own, landing, kv_send.at[phase], kv_recv.at[phase]).wait_send()
+        return c
+
+    lax.fori_loop(1, k_size, finish, 0)
+
+
+def fused(
+    tokens,
+    live_lengths,
+    kv_cache,
+    gate_sums,
+    w_query,
+    w_key,
+    w_value,
+    w_forget,
+    forget_bias,
+    w_out,
+    first_gain,
+    w_gate,
+    w_up,
+    w_down,
+    second_gain,
+):
+    k_size, t_size = lax.axis_size("kv"), lax.axis_size("tp")
+    seqs = tokens.shape[0]
+    positions = kv_cache.shape[1]
+    heads = kv_cache.shape[2] // (2 * DH)
+    rows = heads * GROUP
+    row_n, q_cols = w_query.shape
+    kk = w_key.shape[1]
+    width = w_out.shape[1]
+    ff = w_gate.shape[1]
+    chunk = kk
+    n_chunks = q_cols // chunk + 3
+    f_chunk = -(-ff // (k_size * LANES)) * LANES
+    padded = f_chunk * k_size
+    per = seqs // k_size
+    dims = (seqs, k_size, t_size, heads, chunk, n_chunks, f_chunk, positions)
+    vmem = pl.BlockSpec(memory_space=pltpu.VMEM)
+    smem = pl.BlockSpec(memory_space=pltpu.SMEM)
+    hbm = pl.BlockSpec(memory_space=pl.ANY)
+    V = pltpu.VMEM
+    scratch = [
+        V((row_n, q_cols + 2 * kk), BF16),
+        V((row_n, w_forget.shape[1]), BF16),
+        V(kv_cache.shape, BF16),
+        V(gate_sums.shape, F32),
+        V(w_out.shape, BF16),
+        V((row_n, padded), BF16),
+        V((row_n, padded), BF16),
+        V((padded, width), BF16),
+        V((seqs + 8, LANES), F32),
+        V((t_size, seqs + 8, LANES), F32),
+        V((n_chunks, seqs, chunk), F32),
+        V((k_size, seqs, chunk), F32),
+        V((seqs, chunk), F32),
+        V((k_size, seqs, chunk), F32),
+        V((seqs * rows, LANES), F32),
+        V((seqs * rows, LANES), F32),
+        V((seqs, LANES), F32),
+        V((k_size, per, rows, LANES), F32),
+        V((k_size, per, rows, LANES), F32),
+        V((per * rows, LANES), F32),
+        V((k_size, per * rows, LANES), F32),
+        V((seqs, width), F32),
+        V((t_size, seqs, width), F32),
+        V((seqs, width), F32),
+        V((t_size, seqs, width), F32),
+        V((seqs, LANES), F32),
+        V((k_size, seqs, LANES), F32),
+        V((seqs, LANES), F32),
+        V((k_size, seqs, LANES), F32),
+        V((k_size, 2, seqs, f_chunk), BF16),
+        V((k_size, 2, seqs, f_chunk), BF16),
+        V((seqs, f_chunk), BF16),
+        V((k_size, seqs, f_chunk), BF16),
+        V((seqs, width), F32),
+        pltpu.SemaphoreType.DMA((10,)),
+        pltpu.SemaphoreType.DMA((3, t_size)),
+        pltpu.SemaphoreType.DMA((3, t_size)),
+        pltpu.SemaphoreType.DMA((8, k_size)),
+        pltpu.SemaphoreType.DMA((8, k_size)),
+    ]
+    return pl.pallas_call(
+        functools.partial(fused_kernel, dims),
+        out_shape=jax.ShapeDtypeStruct(tokens.shape, BF16),
+        in_specs=[vmem, smem, hbm, hbm, hbm, hbm, hbm, hbm, vmem, hbm, vmem, hbm, hbm, hbm, vmem],
+        out_specs=vmem,
+        scratch_shapes=scratch,
+        compiler_params=pltpu.CompilerParams(
+            collective_id=0, has_side_effects=True, vmem_limit_bytes=60 * 1024 * 1024
+        ),
+    )(
+        tokens,
+        live_lengths,
+        kv_cache,
+        gate_sums,
+        w_query,
+        w_key,
+        w_value,
+        w_forget,
+        forget_bias.reshape(1, -1),
+        w_out,
+        first_gain.reshape(1, -1),
+        w_gate,
+        w_up,
+        w_down,
+        second_gain.reshape(1, -1),
+    )
+
+
+def fits(tokens, kv_cache, w_query, w_key, w_gate):
+    k_size = lax.axis_size("kv")
+    heads = kv_cache.shape[2] // (2 * DH)
+    return (
+        tokens.shape[1] == LANES
+        and tokens.shape[0] % 16 == 0
+        and tokens.shape[0] % k_size == 0
+        and heads % 2 == 0
+        and w_key.shape[1] % LANES == 0
+        and w_query.shape[1] % w_key.shape[1] == 0
+        and w_query.shape[1] // w_key.shape[1] + 3 <= k_size
+        and w_gate.shape[1] % LANES == 0
+    )
+
+
+def choose(*args):
+    if fits(args[0], args[2], args[4], args[5], args[11]):
+        return fused(*args)
+    return on_device(*args)
+
+
 def solution(mesh):
     in_specs = (
         P(None, ("kv", "tp")),
@@ -160,5 +729,5 @@
     )
     out_specs = P(None, ("kv", "tp"))
     return jax.shard_map(
-        on_device, mesh=mesh, in_specs=in_specs, out_specs=out_specs, check_vma=False
-    )
+        choose, mesh=mesh, in_specs=in_specs, out_specs=out_specs, check_vma=False
+    )

time: 335 us -> 66.7 us (0.20)
  blocking collectives: 203 us -> 0 us
  waiting for transfers between devices: 69.4 us -> 0 us
  Pallas kernels: 0 us -> 63 us
  matrix products: 17.4 us -> 0 us
  local copies, waits for them, and re-layouts: 18 us -> 3.51 us
  between operations: 13.5 us -> 0.01 us
  other arithmetic: 12.2 us -> 0 us
    all_gather x5 -> x0, blocking collectives: 106 us -> none  [the longest x3 94.9 us: combined_all(): everything = jax.tree.map(lambda part: lax.all_gather(part, axis), shard)]
    psum x5 -> x0, blocking collectives: 96.7 us -> none  [the longest x1 39.2 us: on_device(): lax.psum((query_part, key_part, value_part, forget_part), 'kv')]
    psum x1 -> x0, waiting for transfers between devices: 69.4 us -> none  [on_device(): lax.psum(up_part.astype(jnp.bfloat16), 'kv').astype(jnp.float32)]
    pallas_call x0 -> x1, Pallas kernels: none -> 63 us  [fused(): pl.pallas_call(functools.partial(fused_kernel, dims), out_shape=jax.Shape...]
    dot_general x11 -> x0, matrix products: 17.4 us -> none  [the longest x1 3.45 us: on_device(): jnp.einsum('bgjp,bpgd->bgjd', weights.astype(jnp.bfloat16), cached[:, :,...]
    unnamed x15 -> x2, local copies, waits for them, and re-layouts: 14 us -> 3.51 us
    add x15 -> x0, other arithmetic: 9.49 us -> none  [the longest x7 9.26 us: combine_parts(): earlier_sum * earlier_scale[..., None] + later_sum * later_scale[..., None]]
  transfers between devices with their start and end apart: 1 -> 0, of which waited for: 1 -> 0; matrix products, arithmetic and copies ran while one was open for 0% -> 0% of each run, Pallas kernels for 0% -> 0%
where the time goes in v1:
time: 66.7 us; the launch traced here: 66.5 us
  Pallas kernels  63 us (94%)
  local copies, waits for them, and re-layouts  3.51 us (5%)
    pallas_call x1, Pallas kernels, fused(): pl.pallas_call(functools.partial(fused_kernel, dims), out_shape=jax.Shape...  63 us
    unnamed x2, local copies, waits for them, and re-layouts  3.51 us

profile of v1, /device:TPU:0, one launch (start us, length us, event | category | flops | bytes accessed | tf_op | source)
XLA Modules:
  0.0 66.5 jit_solution(15882898445640718108)
XLA Ops:
  0.0 2.2 %copy.16.wf_hbm = bf16[4096,16]{1,0:T(8,128)(2,1)} copy(bf16[4096,16]{0,1:T(8,128)(2,1)} %param.22) | data formatting | bytes 262144 | tf_op args[7]
  2.2 63.0 %shard_map.145 = bf16[16,128]{1,0:T(8,128)(2,1)} custom-call(bf16[16,128]{1,0:T(8,128)(2,1)} %tokens.1, s32[16]{0:T(128)} %lengths.1, bf16[16,512,512]{2,1,0:T(8,128)(2,1)} %cache_hbm.1, f32[16,4,512]{2,1,0:T(4,128)} %gates_hbm.1, bf16[512,1024]{1,0:T(8,128)(2,1)} %wq_hbm.1, bf16[512,256]{1,0:T(8,128)(2,1)} %wk_hbm.1, bf16[512,256]{1,0:T(8,128)(2,1)} %wv_hbm.1, ...), custom_call_target="tpu_custom_call" | custom-call | tf_op jit(solution)/shard_map/pallas_call | solution.py:663
  65.2 1.3 %copy.18 = bf16[16,128]{1,0:T(8,128)(2,1)} copy(bf16[16,128]{1,0:T(8,128)(2,1)} %shard_map.145) | data formatting | bytes 8192

commit v2 on v1

--- a/solution.py
+++ b/solution.py
@@ -159,6 +159,10 @@
         device_id={axis: peer},
         device_id_type=MESH,
     )
+
+
+def partner(m, me, size):
+    return lax.rem(me + 1 + m, size)
 
 
 def arrival(axis, peer, source, landing, sends, recvs):
@@ -209,6 +213,8 @@
     qkv_in,
     qkv_own,
     qkv_all,
+    f_own,
+    f_all,
     q_rows,
     kv_rows,
     gate_now,
@@ -250,7 +256,7 @@
         pltpu.make_async_copy(wk_hbm, wqkv.at[:, q_cols : q_cols + kk], sems.at[1]),
         pltpu.make_async_copy(wv_hbm, wqkv.at[:, q_cols + kk :], sems.at[2]),
         pltpu.make_async_copy(
-            wf_hbm.at[pl.ds(pl.multiple_of(kv * rows_n, rows_n), rows_n), :], wf, sems.at[3]
+            wf_hbm.at[:, pl.ds(pl.multiple_of(kv * rows_n, rows_n), rows_n)], wf, sems.at[3]
         ),
         pltpu.make_async_copy(cache_hbm, cache, sems.at[4]),
         pltpu.make_async_copy(gates_hbm, gates, sems.at[5]),
@@ -259,17 +265,17 @@
         pltpu.make_async_copy(wu_hbm, wu.at[:, :ff], sems.at[8]),
         pltpu.make_async_copy(wd_hbm, wd.at[:ff, :], sems.at[9]),
     ]
-    for copy in local:
-        copy.start()
     barrier = pltpu.get_barrier_semaphore()
-    for i in range(1, k_size):
+    for i in range(k_size - 1):
         pl.semaphore_signal(
-            barrier, inc=1, device_id={"kv": lax.rem(kv + i, k_size)}, device_id_type=MESH
+            barrier, inc=1, device_id={"kv": partner(i, kv, k_size)}, device_id_type=MESH
         )
     for i in range(1, t_size):
         pl.semaphore_signal(
             barrier, inc=1, device_id={"tp": lax.rem(tp + i, t_size)}, device_id_type=MESH
         )
+    for copy in local:
+        copy.start()
     padded = wg.shape[1]
     if padded > ff:
         wg[:, ff:] = jnp.zeros((rows_n, padded - ff), BF16)
@@ -291,16 +297,16 @@
         s, r = kv_send.at[phase], kv_recv.at[phase]
 
         def go(i, c):
-            push("kv", lax.rem(kv + i, k_size), kv, own, landing, s, r).start()
+            push("kv", partner(i, kv, k_size), kv, own, landing, s, r).start()
             return c
 
         def come(i, c):
-            arrival("kv", lax.rem(kv + i, k_size), own, landing, s, r).wait_recv()
+            arrival("kv", partner(i, kv, k_size), own, landing, s, r).wait_recv()
             return c
 
-        lax.fori_loop(1, k_size, go, 0)
+        lax.fori_loop(0, k_size - 1, go, 0)
         landing[kv] = own[...]
-        lax.fori_loop(1, k_size, come, 0)
+        lax.fori_loop(0, k_size - 1, come, 0)
 
     tp_all(0, tok_own, tok_all)
     wide_rows = jnp.concatenate([tok_all[t, :seqs, :] for t in range(t_size)], axis=1)
@@ -313,14 +319,16 @@
         qkv_part[c] = jnp.dot(
             block, wqkv[:, c * chunk : (c + 1) * chunk], preferred_element_type=F32
         )
-    kv_heads = wf.shape[1]
+    kv_heads = wf.shape[0]
     qkv_part[n_chunks - 1] = jnp.zeros((seqs, chunk), F32)
-    qkv_part[n_chunks - 1, :, :kv_heads] = jnp.dot(block, wf[...], preferred_element_type=F32)
+    qkv_part[n_chunks - 1, :, :kv_heads] = lax.dot_general(
+        block, wf[...], (((1,), (1,)), ((), ())), preferred_element_type=F32
+    )
     s, r = kv_send.at[0], kv_recv.at[0]
     s2, r2 = kv_send.at[1], kv_recv.at[1]
 
     def qkv_go(i, c):
-        peer = lax.rem(kv + i, k_size)
+        peer = partner(i, kv, k_size)
 
         @pl.when(peer < n_chunks)
         def _():
@@ -328,47 +336,61 @@
 
         return c
 
-    lax.fori_loop(1, k_size, qkv_go, 0)
+    lax.fori_loop(0, k_size - 1, qkv_go, 0)
 
     @pl.when(kv < n_chunks)
     def _():
         qkv_in[kv] = qkv_part[kv]
 
         def come(i, c):
-            peer = lax.rem(kv + i, k_size)
+            peer = partner(i, kv, k_size)
             arrival("kv", peer, qkv_part.at[0], qkv_in, s, r).wait_recv()
             return c
 
-        lax.fori_loop(1, k_size, come, 0)
+        lax.fori_loop(0, k_size - 1, come, 0)
         total = qkv_in[0]
         for k in range(1, k_size):
             total = total + qkv_in[k]
         scale = jnp.where(kv < q_cols // chunk, DH**-0.5, 1.0).astype(F32)
-        rounded = total.astype(BF16).astype(F32) * scale
-        exact = jnp.full((seqs, chunk), kv, jnp.int32) == n_chunks - 1
-        qkv_own[...] = jnp.where(exact, total, rounded)
-
-        def go(i, c):
-            push("kv", lax.rem(kv + i, k_size), kv, qkv_own, qkv_all, s2, r2).start()
-            return c
-
-        lax.fori_loop(1, k_size, go, 0)
-        qkv_all[kv] = qkv_own[...]
+        qkv_own[...] = (total.astype(BF16).astype(F32) * scale).astype(BF16)
+        f_own[...] = total[:, :LANES]
+
+        @pl.when(kv < n_chunks - 1)
+        def _():
+            def go(i, c):
+                push("kv", partner(i, kv, k_size), kv, qkv_own, qkv_all, s2, r2).start()
+                return c
+
+            lax.fori_loop(0, k_size - 1, go, 0)
+            qkv_all[kv] = qkv_own[...]
+
+        @pl.when(kv == n_chunks - 1)
+        def _():
+            def go(i, c):
+                push("kv", partner(i, kv, k_size), kv, f_own, f_all, s2, r2).start()
+                return c
+
+            lax.fori_loop(0, k_size - 1, go, 0)
+            f_all[kv] = f_own[...]
 
     def qkv_come(i, c):
-        peer = lax.rem(kv + i, k_size)
-
-        @pl.when(peer < n_chunks)
+        peer = partner(i, kv, k_size)
+
+        @pl.when(peer < n_chunks - 1)
         def _():
             arrival("kv", peer, qkv_own, qkv_all, s2, r2).wait_recv()
 
+        @pl.when(peer == n_chunks - 1)
+        def _():
+            arrival("kv", peer, f_own, f_all, s2, r2).wait_recv()
+
         return c
 
-    lax.fori_loop(1, k_size, qkv_come, 0)
+    lax.fori_loop(0, k_size - 1, qkv_come, 0)
     lane = lax.broadcasted_iota(jnp.int32, (seqs, LANES), 1)
 
     def unit(start):
-        return qkv_all[start // chunk, :, start % chunk : start % chunk + LANES]
+        return qkv_all[start // chunk, :, start % chunk : start % chunk + LANES].astype(F32)
 
     for h in range(rows):
         start = h * DH
@@ -384,7 +406,7 @@
         pair = jnp.where(lane < DH, keys, values)
         for j in range(GROUP):
             kv_rows[pl.ds(g * GROUP + j, seqs, stride=rows), :] = pair
-    logits = qkv_all[n_chunks - 1, :, :kv_heads] + bias[...]
+    logits = f_all[n_chunks - 1, :, :kv_heads] + bias[...]
     gate_now[:, :kv_heads] = jnp.minimum(logits, 0.0) - jnp.log(1.0 + jnp.exp(-jnp.abs(logits)))
     local[4].wait()
     local[5].wait()
@@ -429,24 +451,24 @@
     sa, ra = kv_send.at[2], kv_recv.at[2]
 
     def att_go(i, c):
-        peer = lax.rem(kv + i, k_size)
+        peer = partner(i, kv, k_size)
         for e in range(per):
             att_part[peer, e] = attend(peer * per + e)
 
-        @pl.when(i < k_size)
+        @pl.when(i < k_size - 1)
         def _():
             push("kv", peer, kv, att_part.at[peer], att_in, sa, ra).start()
 
         return c
 
-    lax.fori_loop(1, k_size + 1, att_go, 0)
+    lax.fori_loop(0, k_size, att_go, 0)
     att_in[kv] = att_part[kv]
 
     def att_come(i, c):
-        arrival("kv", lax.rem(kv + i, k_size), att_part.at[0], att_in, sa, ra).wait_recv()
+        arrival("kv", partner(i, kv, k_size), att_part.at[0], att_in, sa, ra).wait_recv()
         return c
 
-    lax.fori_loop(1, k_size, att_come, 0)
+    lax.fori_loop(0, k_size - 1, att_come, 0)
     for e in range(per):
         at = pl.ds(pl.multiple_of((kv * per + e) * rows, rows), rows)
         q, pair = q_rows[at, :], kv_rows[at, :]
@@ -463,10 +485,18 @@
             scale = jnp.exp(top - high)
             numer = numer + part * scale
             denom = denom + part[:, DH // 2 : DH // 2 + 1] * scale
-        att_own[pl.ds(e * rows, rows), :] = jnp.where(lane_l < DH, 0.0, numer / denom)
+        done = numer / denom
+        if e % 2 == 0:
+            left = pltpu.roll(done, DH, 1)
+        else:
+            both = jnp.where(lane_l < DH, left, done).astype(BF16)
+            att_own[e // 2 * rows : (e // 2 + 1) * rows, :] = both
     kv_all(3, att_own, att_all)
     for k in range(k_size):
-        q_rows[k * per * rows : (k + 1) * per * rows, :] = att_all[k]
+        for e in range(per):
+            pair = att_all[k, e // 2 * rows : (e // 2 + 1) * rows, :].astype(F32)
+            pair = pltpu.roll(pair, DH, 1) if e % 2 == 0 else pair
+            q_rows[(k * per + e) * rows : (k * per + e + 1) * rows, :] = pair
     pieces = []
     for h in range(0, rows, 2):
         even = pltpu.roll(q_rows[pl.ds(h, seqs, stride=rows), :], DH, 1)
@@ -499,25 +529,25 @@
     sg, rg = kv_send.at[5], kv_recv.at[5]
 
     def gu_go(i, c):
-        peer = lax.rem(kv + i, k_size)
+        peer = partner(i, kv, k_size)
         at = pl.ds(pl.multiple_of(peer * f_chunk, LANES), f_chunk)
         gu_part[peer, 0] = jnp.dot(mid, wg[:, at], preferred_element_type=F32).astype(BF16)
         gu_part[peer, 1] = jnp.dot(mid, wu[:, at], preferred_element_type=F32).astype(BF16)
 
-        @pl.when(i < k_size)
+        @pl.when(i < k_size - 1)
         def _():
             push("kv", peer, kv, gu_part.at[peer], gu_in, sg, rg).start()
 
         return c
 
-    lax.fori_loop(1, k_size + 1, gu_go, 0)
+    lax.fori_loop(0, k_size, gu_go, 0)
     gu_in[kv] = gu_part[kv]
 
     def gu_come(i, c):
-        arrival("kv", lax.rem(kv + i, k_size), gu_part.at[0], gu_in, sg, rg).wait_recv()
+        arrival("kv", partner(i, kv, k_size), gu_part.at[0], gu_in, sg, rg).wait_recv()
         return c
 
-    lax.fori_loop(1, k_size, gu_come, 0)
+    lax.fori_loop(0, k_size - 1, gu_come, 0)
     gate = gu_in[0, 0].astype(F32)
     up = gu_in[0, 1].astype(F32)
     for k in range(1, k_size):
@@ -528,10 +558,10 @@
     sh, rh = kv_send.at[6], kv_recv.at[6]
 
     def hid_go(i, c):
-        push("kv", lax.rem(kv + i, k_size), kv, hid_own, hid_all, sh, rh).start()
+        push("kv", partner(i, kv, k_size), kv, hid_own, hid_all, sh, rh).start()
         return c
 
-    lax.fori_loop(1, k_size, hid_go, 0)
+    lax.fori_loop(0, k_size - 1, hid_go, 0)
     hid_all[kv] = hid_own[...]
 
     def down(i, acc):
@@ -559,15 +589,19 @@
             arrival("tp", peer, own, landing, tp_send.at[phase], tp_recv.at[phase]).wait_send()
 
     def finish(i, c):
-        peer = lax.rem(kv + i, k_size)
+        peer = partner(i, kv, k_size)
 
         @pl.when(peer < n_chunks)
         def _():
             arrival("kv", peer, qkv_part.at[peer], qkv_in, s, r).wait_send()
 
-        @pl.when(kv < n_chunks)
+        @pl.when(kv < n_chunks - 1)
         def _():
             arrival("kv", peer, qkv_own, qkv_all, s2, r2).wait_send()
+
+        @pl.when(kv == n_chunks - 1)
+        def _():
+            arrival("kv", peer, f_own, f_all, s2, r2).wait_send()
 
         for phase, own, landing in (
             (2, att_part.at[peer], att_in),
@@ -580,7 +614,7 @@
             arrival("kv", peer, own, landing, kv_send.at[phase], kv_recv.at[phase]).wait_send()
         return c
 
-    lax.fori_loop(1, k_size, finish, 0)
+    lax.fori_loop(0, k_size - 1, finish, 0)
 
 
 def fused(
@@ -621,7 +655,7 @@
     V = pltpu.VMEM
     scratch = [
         V((row_n, q_cols + 2 * kk), BF16),
-        V((row_n, w_forget.shape[1]), BF16),
+        V((w_forget.shape[1], row_n), BF16),
         V(kv_cache.shape, BF16),
         V(gate_sums.shape, F32),
         V(w_out.shape, BF16),
@@ -632,15 +666,17 @@
         V((t_size, seqs + 8, LANES), F32),
         V((n_chunks, seqs, chunk), F32),
         V((k_size, seqs, chunk), F32),
-        V((seqs, chunk), F32),
-        V((k_size, seqs, chunk), F32),
+        V((seqs, chunk), BF16),
+        V((k_size, seqs, chunk), BF16),
+        V((seqs, LANES), F32),
+        V((k_size, seqs, LANES), F32),
         V((seqs * rows, LANES), F32),
         V((seqs * rows, LANES), F32),
         V((seqs, LANES), F32),
         V((k_size, per, rows, LANES), F32),
         V((k_size, per, rows, LANES), F32),
-        V((per * rows, LANES), F32),
-        V((k_size, per * rows, LANES), F32),
+        V((per // 2 * rows, LANES), BF16),
+        V((k_size, per // 2 * rows, LANES), BF16),
         V((seqs, width), F32),
         V((t_size, seqs, width), F32),
         V((seqs, width), F32),
@@ -677,7 +713,7 @@
         w_query,
         w_key,
         w_value,
-        w_forget,
+        w_forget.T,
         forget_bias.reshape(1, -1),
         w_out,
         first_gain.reshape(1, -1),
@@ -694,7 +730,8 @@
     return (
         tokens.shape[1] == LANES
         and tokens.shape[0] % 16 == 0
-        and tokens.shape[0] % k_size == 0
+        and tokens.shape[0] % (2 * k_size) == 0
+        and k_size % 2 == 0
         and heads % 2 == 0
         and w_key.shape[1] % LANES == 0
         and w_query.shape[1] % w_key.shape[1] == 0

time: 66.7 us -> 63.5 us (0.952)
  local copies, waits for them, and re-layouts: 3.51 us -> 1.28 us
  Pallas kernels: 63 us -> 62 us
    unnamed x2 -> x1, local copies, waits for them, and re-layouts: 3.51 us -> 1.28 us
    pallas_call x1, Pallas kernels: 63 us -> 62 us  [fused(): pl.pallas_call(functools.partial(fused_kernel, dims), out_shape=jax.Shape...]
where the time goes in v2:
time: 63.5 us; the launch traced here: 63.3 us
  Pallas kernels  62 us (98%)
  local copies, waits for them, and re-layouts  1.28 us (2%)
    pallas_call x1, Pallas kernels, fused(): pl.pallas_call(functools.partial(fused_kernel, dims), out_shape=jax.Shape...  62 us
    unnamed x1, local copies, waits for them, and re-layouts  1.28 us

profile of v2, /device:TPU:0, one launch (start us, length us, event | category | flops | bytes accessed | tf_op | source)
XLA Modules:
  0.0 63.3 jit_solution(12185321372256154231)
XLA Ops:
  0.0 62.0 %shard_map.145 = bf16[16,128]{1,0:T(8,128)(2,1)} custom-call(bf16[16,128]{1,0:T(8,128)(2,1)} %tokens.1, s32[16]{0:T(128)} %lengths.1, bf16[16,512,512]{2,1,0:T(8,128)(2,1)} %cache_hbm.1, f32[16,4,512]{2,1,0:T(4,128)} %gates_hbm.1, bf16[512,1024]{1,0:T(8,128)(2,1)} %wq_hbm.1, bf16[512,256]{1,0:T(8,128)(2,1)} %wk_hbm.1, bf16[512,256]{1,0:T(8,128)(2,1)} %wv_hbm.1, ...), custom_call_target="tpu_custom_call" | custom-call | tf_op jit(solution)/shard_map/pallas_call | solution.py:699
  62.0 1.3 %copy.17 = bf16[16,128]{1,0:T(8,128)(2,1)} copy(bf16[16,128]{1,0:T(8,128)(2,1)} %shard_map.145) | data formatting | bytes 8192

commit v3 on v2

--- a/solution.py
+++ b/solution.py
@@ -232,6 +232,8 @@
     s2_in,
     gu_part,
     gu_in,
+    g_part,
+    g_in,
     hid_own,
     hid_all,
     wide,
@@ -463,6 +465,27 @@
 
     lax.fori_loop(0, k_size, att_go, 0)
     att_in[kv] = att_part[kv]
+    local[7].wait()
+    local[8].wait()
+    gain_block = jnp.broadcast_to(wide_gain, (seqs, width)).astype(BF16)
+    first_row = lax.broadcasted_iota(jnp.int32, (8, f_chunk), 0) == 0
+    sc, rc = kv_send.at[8], kv_recv.at[8]
+
+    def gain_go(i, c):
+        peer = partner(i, kv, k_size)
+        at = pl.ds(pl.multiple_of(peer * f_chunk, LANES), f_chunk)
+        through_gate = jnp.dot(gain_block, wg[:, at], preferred_element_type=F32)
+        through_up = jnp.dot(gain_block, wu[:, at], preferred_element_type=F32)
+        g_part[peer] = jnp.where(first_row, through_gate[:8], through_up[:8])
+
+        @pl.when(i < k_size - 1)
+        def _():
+            push("kv", peer, kv, g_part.at[peer], g_in, sc, rc).start()
+
+        return c
+
+    lax.fori_loop(0, k_size, gain_go, 0)
+    g_in[kv] = g_part[kv]
 
     def att_come(i, c):
         arrival("kv", partner(i, kv, k_size), att_part.at[0], att_in, sa, ra).wait_recv()
@@ -523,16 +546,25 @@
     z = wide[...]
     for t in range(t_size):
         z = z + x_in[t]
-    mid = (normed(z, 4, s1_own, s1_in) * wide_gain).astype(BF16)
-    local[7].wait()
-    local[8].wait()
+    block_mean = jnp.sum(z, axis=1, keepdims=True) / width
+    offset = z - block_mean
+    s1_own[...] = jnp.where(lane == 0, block_mean, jnp.sum(offset * offset, axis=1, keepdims=True))
+    ss, rs = kv_send.at[4], kv_recv.at[4]
+
+    def stat_go(i, c):
+        push("kv", partner(i, kv, k_size), kv, s1_own, s1_in, ss, rs).start()
+        return c
+
+    lax.fori_loop(0, k_size - 1, stat_go, 0)
+    s1_in[kv] = s1_own[...]
+    lifted = (offset * wide_gain).astype(BF16)
     sg, rg = kv_send.at[5], kv_recv.at[5]
 
     def gu_go(i, c):
         peer = partner(i, kv, k_size)
         at = pl.ds(pl.multiple_of(peer * f_chunk, LANES), f_chunk)
-        gu_part[peer, 0] = jnp.dot(mid, wg[:, at], preferred_element_type=F32).astype(BF16)
-        gu_part[peer, 1] = jnp.dot(mid, wu[:, at], preferred_element_type=F32).astype(BF16)
+        gu_part[peer, 0] = jnp.dot(lifted, wg[:, at], preferred_element_type=F32).astype(BF16)
+        gu_part[peer, 1] = jnp.dot(lifted, wu[:, at], preferred_element_type=F32).astype(BF16)
 
         @pl.when(i < k_size - 1)
         def _():
@@ -547,12 +579,36 @@
         arrival("kv", partner(i, kv, k_size), gu_part.at[0], gu_in, sg, rg).wait_recv()
         return c
 
+    def stat_come(i, c):
+        peer = partner(i, kv, k_size)
+        arrival("kv", peer, s1_own, s1_in, ss, rs).wait_recv()
+        arrival("kv", peer, g_part.at[0], g_in, sc, rc).wait_recv()
+        return c
+
+    lax.fori_loop(0, k_size - 1, stat_come, 0)
+    means = [s1_in[k][:, 0:1] for k in range(k_size)]
+    centre = means[0]
+    for k in range(1, k_size):
+        centre = centre + means[k]
+    centre = centre / k_size
+    shifts = [mean - centre for mean in means]
+    square = jnp.zeros((seqs, 1), F32)
+    for k in range(k_size):
+        square = square + s1_in[k][:, 1:2] + width * shifts[k] * shifts[k]
+    inverse = lax.rsqrt(square / (k_size * width) + EPSILON)
+    mid = ((z - centre) * inverse * wide_gain).astype(BF16)
+    gate = jnp.zeros((seqs, f_chunk), F32)
+    up = jnp.zeros((seqs, f_chunk), F32)
+    for k in range(k_size):
+        through = g_in[k]
+        gate = gate + shifts[k] * through[0:1]
+        up = up + shifts[k] * through[1:2]
     lax.fori_loop(0, k_size - 1, gu_come, 0)
-    gate = gu_in[0, 0].astype(F32)
-    up = gu_in[0, 1].astype(F32)
-    for k in range(1, k_size):
+    for k in range(k_size):
         gate = gate + gu_in[k, 0].astype(F32)
         up = up + gu_in[k, 1].astype(F32)
+    gate = gate * inverse
+    up = up * inverse
     hid_own[...] = (gate / (1.0 + jnp.exp(-gate)) * up).astype(BF16)
     local[9].wait()
     sh, rh = kv_send.at[6], kv_recv.at[6]
@@ -610,6 +666,7 @@
             (5, gu_part.at[peer], gu_in),
             (6, hid_own, hid_all),
             (7, s2_own, s2_in),
+            (8, g_part.at[peer], g_in),
         ):
             arrival("kv", peer, own, landing, kv_send.at[phase], kv_recv.at[phase]).wait_send()
         return c
@@ -687,14 +744,16 @@
         V((k_size, seqs, LANES), F32),
         V((k_size, 2, seqs, f_chunk), BF16),
         V((k_size, 2, seqs, f_chunk), BF16),
+        V((k_size, 8, f_chunk), F32),
+        V((k_size, 8, f_chunk), F32),
         V((seqs, f_chunk), BF16),
         V((k_size, seqs, f_chunk), BF16),
         V((seqs, width), F32),
         pltpu.SemaphoreType.DMA((10,)),
         pltpu.SemaphoreType.DMA((3, t_size)),
         pltpu.SemaphoreType.DMA((3, t_size)),
-        pltpu.SemaphoreType.DMA((8, k_size)),
-        pltpu.SemaphoreType.DMA((8, k_size)),
+        pltpu.SemaphoreType.DMA((9, k_size)),
+        pltpu.SemaphoreType.DMA((9, k_size)),
     ]
     return pl.pallas_call(
         functools.partial(fused_kernel, dims),

time: 63.5 us -> 60.8 us (0.957)
  Pallas kernels: 62 us -> 59.4 us
    pallas_call x1, Pallas kernels: 62 us -> 59.4 us  [fused(): pl.pallas_call(functools.partial(fused_kernel, dims), out_shape=jax.Shape...]
where the time goes in v3:
time: 60.8 us; the launch traced here: 60.6 us
  Pallas kernels  59.4 us (98%)
  local copies, waits for them, and re-layouts  1.28 us (2%)
    pallas_call x1, Pallas kernels, fused(): pl.pallas_call(functools.partial(fused_kernel, dims), out_shape=jax.Shape...  59.4 us
    unnamed x1, local copies, waits for them, and re-layouts  1.28 us

profile of v3, /device:TPU:0, one launch (start us, length us, event | category | flops | bytes accessed | tf_op | source)
XLA Modules:
  0.0 60.6 jit_solution(5983451258668170964)
XLA Ops:
  0.0 59.4 %shard_map.145 = bf16[16,128]{1,0:T(8,128)(2,1)} custom-call(bf16[16,128]{1,0:T(8,128)(2,1)} %tokens.1, s32[16]{0:T(128)} %lengths.1, bf16[16,512,512]{2,1,0:T(8,128)(2,1)} %cache_hbm.1, f32[16,4,512]{2,1,0:T(4,128)} %gates_hbm.1, bf16[512,1024]{1,0:T(8,128)(2,1)} %wq_hbm.1, bf16[512,256]{1,0:T(8,128)(2,1)} %wk_hbm.1, bf16[512,256]{1,0:T(8,128)(2,1)} %wv_hbm.1, ...), custom_call_target="tpu_custom_call" | custom-call | tf_op jit(solution)/shard_map/pallas_call | solution.py:758
  59.4 1.3 %copy.17 = bf16[16,128]{1,0:T(8,128)(2,1)} copy(bf16[16,128]{1,0:T(8,128)(2,1)} %shard_map.145) | data formatting | bytes 8192

commit v4 on v3

--- a/solution.py
+++ b/solution.py
@@ -388,6 +388,27 @@
 
         return c
 
+    local[7].wait()
+    local[8].wait()
+    gain_block = jnp.broadcast_to(wide_gain, (seqs, width)).astype(BF16)
+    first_row = lax.broadcasted_iota(jnp.int32, (8, f_chunk), 0) == 0
+    sc, rc = kv_send.at[8], kv_recv.at[8]
+
+    def gain_go(i, c):
+        peer = partner(i, kv, k_size)
+        at = pl.ds(pl.multiple_of(peer * f_chunk, LANES), f_chunk)
+        through_gate = jnp.dot(gain_block, wg[:, at], preferred_element_type=F32)
+        through_up = jnp.dot(gain_block, wu[:, at], preferred_element_type=F32)
+        g_part[peer] = jnp.where(first_row, through_gate[:8], through_up[:8])
+
+        @pl.when(i < k_size - 1)
+        def _():
+            push("kv", peer, kv, g_part.at[peer], g_in, sc, rc).start()
+
+        return c
+
+    lax.fori_loop(0, k_size, gain_go, 0)
+    g_in[kv] = g_part[kv]
     lax.fori_loop(0, k_size - 1, qkv_come, 0)
     lane = lax.broadcasted_iota(jnp.int32, (seqs, LANES), 1)
 
@@ -465,27 +486,6 @@
 
     lax.fori_loop(0, k_size, att_go, 0)
     att_in[kv] = att_part[kv]
-    local[7].wait()
-    local[8].wait()
-    gain_block = jnp.broadcast_to(wide_gain, (seqs, width)).astype(BF16)
-    first_row = lax.broadcasted_iota(jnp.int32, (8, f_chunk), 0) == 0
-    sc, rc = kv_send.at[8], kv_recv.at[8]
-
-    def gain_go(i, c):
-        peer = partner(i, kv, k_size)
-        at = pl.ds(pl.multiple_of(peer * f_chunk, LANES), f_chunk)
-        through_gate = jnp.dot(gain_block, wg[:, at], preferred_element_type=F32)
-        through_up = jnp.dot(gain_block, wu[:, at], preferred_element_type=F32)
-        g_part[peer] = jnp.where(first_row, through_gate[:8], through_up[:8])
-
-        @pl.when(i < k_size - 1)
-        def _():
-            push("kv", peer, kv, g_part.at[peer], g_in, sc, rc).start()
-
-        return c
-
-    lax.fori_loop(0, k_size, gain_go, 0)
-    g_in[kv] = g_part[kv]
 
     def att_come(i, c):
         arrival("kv", partner(i, kv, k_size), att_part.at[0], att_in, sa, ra).wait_recv()

time: 60.8 us -> 60.9 us (level)
  no operation moved by 1% of the time
where the time goes in v4:
time: 60.9 us; the launch traced here: 60.7 us
  Pallas kernels  59.5 us (98%)
  local copies, waits for them, and re-layouts  1.28 us (2%)
    pallas_call x1, Pallas kernels, fused(): pl.pallas_call(functools.partial(fused_kernel, dims), out_shape=jax.Shape...  59.5 us
    unnamed x1, local copies, waits for them, and re-layouts  1.28 us

profile of v4, /device:TPU:0, one launch (start us, length us, event | category | flops | bytes accessed | tf_op | source)
XLA Modules:
  0.0 60.7 jit_solution(7809861443597289305)
XLA Ops:
  0.0 59.5 %shard_map.145 = bf16[16,128]{1,0:T(8,128)(2,1)} custom-call(bf16[16,128]{1,0:T(8,128)(2,1)} %tokens.1, s32[16]{0:T(128)} %lengths.1, bf16[16,512,512]{2,1,0:T(8,128)(2,1)} %cache_hbm.1, f32[16,4,512]{2,1,0:T(4,128)} %gates_hbm.1, bf16[512,1024]{1,0:T(8,128)(2,1)} %wq_hbm.1, bf16[512,256]{1,0:T(8,128)(2,1)} %wk_hbm.1, bf16[512,256]{1,0:T(8,128)(2,1)} %wv_hbm.1, ...), custom_call_target="tpu_custom_call" | custom-call | tf_op jit(solution)/shard_map/pallas_call | solution.py:758
  59.5 1.3 %copy.17 = bf16[16,128]{1,0:T(8,128)(2,1)} copy(bf16[16,128]{1,0:T(8,128)(2,1)} %shard_map.145) | data formatting | bytes 8192
